TPU v7x, 512 devices: a whole 4x4x16 slice. The times are simulated.
512 devices in a mesh: kv: 64 (over z, y), tp: 8 (over x, core).
Axes of the slice: x: 4, y: 4, z: 16, core: 2. Of those that a mesh axis runs over, the one named last changes fastest.
Arguments:
- queries: bfloat16 [57344, 1024], P('kv', 'tp'), may hold values from -6 to 6
- keyvals: bfloat16 [57344, 128], P('kv'), may hold values from -6 to 6
- log_sums: float32 [16, 57344], P('tp', 'kv'), may hold values from 6 to 7.2
- out_grad: bfloat16 [57344, 1024], P('kv', 'tp'), may hold values from -24 to 24
- inputs: bfloat16 [57344, 2048], P('kv'), may hold values from -0.3125 to 0.3125
- selection: int32 [448, 16], replicated, may hold values from -1 to 1791, as said below
Outputs:
- query_grad: bfloat16 [57344, 1024], P('kv', 'tp')
- keyval_grad: float32 [1792, 32, 128], P('kv', 'tp')
- weight_grad: float32 [2048, 1024], P('kv', 'tp')
Inputs may be any that keep to these rules, and one draw needn't show every extreme that they name: `selection`: row j first names the key blocks of query block j's own positions in order, then distinct blocks of earlier devices' positions, then -1 entries at the end (only where fewer earlier blocks exist). The rows of one device's query blocks together name at most 2 distinct blocks of any one other device, and exactly 2 for some pair in every draw.
All inputs are finite; a program needn't handle non-finite values.
Results may differ from a plain program's by a relative error of at most 0.0071.
Values may be sent and summed in bfloat16 or wider, within the bound.
No kernel may reach another device: no remote copies, remote signals or barrier semaphores. Data moves between devices by JAX's collectives and lax.ppermute only.
A program may use at most 64 MiB of HBM per device.

v0:
```python
import jax
import jax.numpy as jnp
from jax import lax
from jax.sharding import PartitionSpec as P

DH = 64
QB = 128
KB = 32
NSEL = 16
CAP = 2


def in_blocks(array, dim, peers):
    before, after = (array.shape[:dim], array.shape[dim + 1 :])
    return jnp.moveaxis(array.reshape(*before, peers, -1, *after), dim, 0)


def sum_at_owner(array, axis, dim):
    peers = lax.axis_size(axis)
    blocks = lax.all_to_all(in_blocks(array, dim, peers), axis, 0, 0, tiled=True)
    return jnp.sum(blocks.astype(jnp.float32), axis=0)


def slot_table(wanted):
    slot_rank = jnp.cumsum(wanted.astype(jnp.int32), axis=1) - 1
    return wanted[:, None, :] & (
        slot_rank[:, None, :] == jnp.arange(CAP, dtype=jnp.int32)[None, :, None]
    )


def weight_term(inputs, query_grad):
    return lax.dot_general(
        inputs, query_grad, (((0,), (0,)), ((), ())), preferred_element_type=jnp.float32
    )


def body(queries, keyvals, log_sums, out_grad, inputs, selection):
    kv_count = lax.axis_size("kv")
    own_index = lax.axis_index("kv")
    tok_count, width = queries.shape
    head_count = width // DH
    per_dev = tok_count // QB
    own_blocks = tok_count // KB
    slot_count = kv_count * CAP
    score_scale = DH ** (-0.5)
    own_kv = keyvals.reshape(own_blocks, KB, 2 * DH)
    lists = selection.reshape(kv_count, per_dev * NSEL)
    device_ids = jnp.arange(kv_count, dtype=jnp.int32)
    mine = own_index * own_blocks + jnp.arange(own_blocks, dtype=jnp.int32)
    wanted = jnp.any(lists[:, :, None] == mine[None, None, :], axis=1) & (
        device_ids[:, None] != own_index
    )
    owner_slots = slot_table(wanted)
    outgoing = jnp.einsum(
        "rsb,bkc->rskc",
        owner_slots.astype(jnp.bfloat16),
        own_kv,
        preferred_element_type=jnp.float32,
    ).astype(jnp.bfloat16)
    fetched = lax.all_to_all(outgoing, "kv", split_axis=0, concat_axis=0, tiled=True)
    block_list = lax.dynamic_index_in_dim(lists, own_index, 0, keepdims=False)
    every_block = jnp.arange(kv_count * own_blocks, dtype=jnp.int32)
    hits = block_list[:, None] == every_block[None, :]
    needed = jnp.any(hits, axis=0).reshape(kv_count, own_blocks) & (
        device_ids[:, None] != own_index
    )
    slot_rank = jnp.cumsum(needed.astype(jnp.int32), axis=1) - 1
    entry_rank = jnp.sum(jnp.where(hits, slot_rank.reshape(-1)[None, :], 0), axis=1)
    safe_list = jnp.maximum(block_list, 0)
    owner_index = safe_list // own_blocks
    local_block = safe_list % own_blocks
    pool_index = jnp.where(
        owner_index == own_index, slot_count + local_block, owner_index * CAP + entry_rank
    )
    pool_index = jnp.where(block_list < 0, 0, pool_index)
    block_pool = jnp.concatenate([fetched.reshape(slot_count, KB, 2 * DH), own_kv], axis=0)
    gathered = jnp.take(block_pool, pool_index, axis=0).reshape(per_dev, NSEL * KB, 2 * DH)
    key_rows = gathered[:, :, :DH]
    value_rows = gathered[:, :, DH:]
    query_rows = queries.reshape(per_dev, QB, head_count, DH)
    grad_rows = out_grad.reshape(per_dev, QB, head_count, DH)
    log_rows = log_sums.reshape(head_count, per_dev, QB).transpose(1, 0, 2)
    key_pos = (
        safe_list.reshape(per_dev, NSEL, 1) * KB + jnp.arange(KB, dtype=jnp.int32)[None, None, :]
    ).reshape(per_dev, NSEL * KB)
    key_live = jnp.repeat((block_list >= 0).reshape(per_dev, NSEL), KB, axis=1)
    query_pos = own_index * tok_count + jnp.arange(tok_count, dtype=jnp.int32).reshape(per_dev, QB)
    live_mask = key_live[:, None, :] & (key_pos[:, None, :] <= query_pos[:, :, None])
    scores = (
        jnp.einsum("pthd,pkd->phtk", query_rows, key_rows, preferred_element_type=jnp.float32)
        * score_scale
    )
    prob_f32 = jnp.where(live_mask[:, None], jnp.exp(scores - log_rows[..., None]), 0.0)
    prob_b = prob_f32.astype(jnp.bfloat16)
    recomputed = jnp.einsum(
        "phtk,pkd->pthd", prob_b, value_rows, preferred_element_type=jnp.float32
    )
    row_delta = jnp.sum(grad_rows.astype(jnp.float32) * recomputed, axis=-1)
    dprob = jnp.einsum("pthd,pkd->phtk", grad_rows, value_rows, preferred_element_type=jnp.float32)
    dscore = prob_f32 * (dprob - row_delta.transpose(0, 2, 1)[..., None])
    dscore_b = dscore.astype(jnp.bfloat16)
    query_grad = (
        (
            jnp.einsum("phtk,pkd->pthd", dscore_b, key_rows, preferred_element_type=jnp.float32)
            * score_scale
        )
        .astype(jnp.bfloat16)
        .reshape(tok_count, width)
    )
    key_grad = (
        jnp.einsum("phtk,pthd->pkd", dscore_b, query_rows, preferred_element_type=jnp.float32)
        * score_scale
    )
    value_grad = jnp.einsum("phtk,pthd->pkd", prob_b, grad_rows, preferred_element_type=jnp.float32)
    entry_grads = jnp.concatenate([key_grad, value_grad], axis=-1).reshape(
        per_dev * NSEL, KB, 2 * DH
    )
    spread = (
        pool_index[:, None] == jnp.arange(slot_count + own_blocks, dtype=jnp.int32)[None, :]
    ).astype(jnp.float32)
    shares = sum_at_owner(entry_grads.astype(jnp.bfloat16), "tp", 1)
    summed = jnp.einsum("ep,ekc->pkc", spread, shares, precision=lax.Precision.HIGHEST)
    key_share = summed.shape[1]
    returned = lax.all_to_all(
        summed[:slot_count].reshape(kv_count, CAP, key_share, 2 * DH).astype(jnp.bfloat16),
        "kv",
        split_axis=0,
        concat_axis=0,
        tiled=True,
    ).astype(jnp.float32)
    keyval_grad = (
        jnp.einsum(
            "rsb,rskc->bkc",
            owner_slots.astype(jnp.float32),
            returned,
            precision=lax.Precision.HIGHEST,
        )
        + summed[slot_count:]
    )
    weight_grad = sum_at_owner(weight_term(inputs, query_grad).astype(jnp.bfloat16), "kv", 0)
    return (query_grad, keyval_grad, weight_grad)


def solution(mesh):
    return jax.shard_map(
        body,
        mesh=mesh,
        in_specs=(P("kv", "tp"), P("kv", None), P("tp", "kv"), P("kv", "tp"), P("kv", None), P()),
        out_specs=(P("kv", "tp"), P("kv", "tp", None), P("kv", "tp")),
        check_vma=False,
    )
```

profile of v0, /device:TPU:8, one launch (start us, length us, event | category | flops | bytes accessed | tf_op | source)
XLA Modules:
  0.0 174.9 jit_solution(13428115641139634798)
XLA Ops:
  0.6 0.9 copy.103
  4.4 1.5 convolution_convert_fusion.1
  5.8 1.7 copy.109
  7.5 18.7 %all-to-all-start = ((bf16[64,2,32,128]{3,2,1,0:T(8,128)(2,1)}), bf16[64,2,32,128]{3,2,1,0:T(8,128)(2,1)S(1)}, u32[]{:S(2)}, u32[]{:S(2)}) async-start(bf16[64,2,32,128]{3,2,1,0:T(8,128)(2,1)} %copy.109), calls=%async_computation | async-start | bytes 2097152 | tf_op jit(solution)/shard_map/all_to_all | solution.py:60
  26.5 0.9 copy.112
  29.0 1.3 copy.115
  31.0 1.3 compare_and_fusion
  32.2 49.2 %all-to-all-done = bf16[64,2,32,128]{3,2,1,0:T(8,128)(2,1)S(1)} async-done(((bf16[64,2,32,128]{3,2,1,0:T(8,128)(2,1)}), bf16[64,2,32,128]{3,2,1,0:T(8,128)(2,1)S(1)}, u32[]{:S(2)}, u32[]{:S(2)}) %all-to-all-start) | async-done | bytes 1048608 | tf_op jit(solution)/shard_map/all_to_all | solution.py:60
  83.6 0.9 fusion.11
  84.6 0.9 fusion.8
  85.5 1.4 fusion.1
  87.6 1.0 pad_maximum_fusion.1
  88.6 2.2 %copy.124 = bf16[7,512,128]{2,1,0:T(8,128)(2,1)} copy(bf16[7,512,128]{1,2,0:T(8,128)(2,1)} %pad_maximum_fusion.1) | data formatting | bytes 1835008 | tf_op jit(solution)/shard_map/concatenate | solution.py:115
  90.8 2.5 %copy.125 = bf16[8,112,4,128]{3,2,1,0:T(4,128)(2,1)} copy(bf16[8,112,4,128]{3,2,0,1:T(4,128)(2,1)} %bitcast.132) | data formatting | bytes 1835008 | tf_op jit(solution)/shard_map/transpose | solution.py:15
  93.3 4.3 %all-to-all-start.1 = ((bf16[8,112,4,128]{3,2,1,0:T(4,128)(2,1)}), bf16[8,112,4,128]{3,2,1,0:T(4,128)(2,1)}, u32[]{:S(2)}, u32[]{:S(2)}) async-start(bf16[8,112,4,128]{3,2,1,0:T(4,128)(2,1)} %copy.125), calls=%async_computation.1 | async-start | bytes 1835008 | tf_op jit(solution)/shard_map/all_to_all | solution.py:20
  97.6 14.6 %all-to-all-done.1 = bf16[8,112,4,128]{3,2,1,0:T(4,128)(2,1)} async-done(((bf16[8,112,4,128]{3,2,1,0:T(4,128)(2,1)}), bf16[8,112,4,128]{3,2,1,0:T(4,128)(2,1)}, u32[]{:S(2)}, u32[]{:S(2)}) %all-to-all-start.1) | async-done | bytes 917536 | tf_op jit(solution)/shard_map/all_to_all | solution.py:20
  112.2 1.3 convert_reduce_fusion
  114.6 6.0 %all-to-all-start.2 = ((bf16[64,2,4,128]{3,1,2,0:T(2,128)(2,1)}), bf16[64,2,4,128]{3,1,2,0:T(2,128)(2,1)S(1)}, u32[]{:S(2)}, u32[]{:S(2)}) async-start(bf16[64,2,4,128]{3,1,2,0:T(2,128)(2,1)} %copy.129), calls=%async_computation.2 | async-start | bytes 262144 | tf_op jit(solution)/shard_map/all_to_all | solution.py:124
  121.2 2.8 %fusion.5 = bf16[2048,128]{0,1:T(8,128)(2,1)S(1)} fusion(bf16[896,128]{0,1:T(8,128)(2,1)S(1)} %bitcast.134, bf16[896,2048]{1,0:T(8,128)(2,1)} %param.10), kind=kOutput, calls=%fused_computation.9 | convolution fusion | flops 470024192 | bytes 4423680 | tf_op jit(solution)/shard_map/dot_general | solution.py:32
  123.9 1.0 copy.131
  124.9 11.8 %all-to-all-done.2 = bf16[64,2,4,128]{3,1,2,0:T(2,128)(2,1)S(1)} async-done(((bf16[64,2,4,128]{3,1,2,0:T(2,128)(2,1)}), bf16[64,2,4,128]{3,1,2,0:T(2,128)(2,1)S(1)}, u32[]{:S(2)}, u32[]{:S(2)}) %all-to-all-start.2) | async-done | bytes 131104 | tf_op jit(solution)/shard_map/all_to_all | solution.py:124
  136.8 5.6 %all-to-all-start.3 = ((bf16[64,32,128]{2,1,0:T(8,128)(2,1)}), bf16[64,32,128]{2,1,0:T(8,128)(2,1)S(1)}, u32[]{:S(2)}, u32[]{:S(2)}) async-start(bf16[64,32,128]{2,1,0:T(8,128)(2,1)} %bitcast.36), calls=%async_computation.3 | async-start | bytes 1048576 | tf_op jit(solution)/shard_map/all_to_all | solution.py:20
  142.4 0.8 copy.132
  144.1 30.1 %all-to-all-done.3 = bf16[64,32,128]{2,1,0:T(8,128)(2,1)S(1)} async-done(((bf16[64,32,128]{2,1,0:T(8,128)(2,1)}), bf16[64,32,128]{2,1,0:T(8,128)(2,1)S(1)}, u32[]{:S(2)}, u32[]{:S(2)}) %all-to-all-start.3) | async-done | bytes 524320 | tf_op jit(solution)/shard_map/all_to_all | solution.py:20
  (73 shorter events, 11.3 us)
Async XLA Ops:
  0.6 25.6 %copy-start.1 = (bf16[896,128]{1,0:T(8,128)(2,1)S(1)}, bf16[896,128]{1,0:T(8,128)(2,1)}, u32[]{:S(2)}) copy-start(bf16[896,128]{1,0:T(8,128)(2,1)} %param.6) | copy-start | bytes 688132
  4.3 24.5 %copy-start.2 = (bf16[896,128]{1,0:T(8,128)(2,1)S(1)}, bf16[896,128]{1,0:T(8,128)(2,1)}, u32[]{:S(2)}) copy-start(bf16[896,128]{1,0:T(8,128)(2,1)} %param.9) | copy-start | bytes 688132
  5.8 24.4 %copy-start.5 = (f32[2,896]{1,0:T(2,128)S(1)}, f32[2,896]{1,0:T(2,128)}, u32[]{:S(2)}) copy-start(f32[2,896]{1,0:T(2,128)} %param.8) | copy-start | bytes 21508
  5.8 75.6 %copy-start = (bf16[896,128]{1,0:T(8,128)(2,1)S(1)}, bf16[896,128]{1,0:T(8,128)(2,1)}, u32[]{:S(2)}) copy-start(bf16[896,128]{1,0:T(8,128)(2,1)} %param.7) | copy-start | bytes 688132
  7.5 73.9 %all-to-all-start = ((bf16[64,2,32,128]{3,2,1,0:T(8,128)(2,1)}), bf16[64,2,32,128]{3,2,1,0:T(8,128)(2,1)S(1)}, u32[]{:S(2)}, u32[]{:S(2)}) async-start(bf16[64,2,32,128]{3,2,1,0:T(8,128)(2,1)} %copy.109), calls=%async_computation | async-start | bytes 2097152 | tf_op jit(solution)/shard_map/all_to_all | solution.py:60
  82.3 1.3 copy-start.3
  84.6 0.9 copy-start.4
  93.3 18.9 %all-to-all-start.1 = ((bf16[8,112,4,128]{3,2,1,0:T(4,128)(2,1)}), bf16[8,112,4,128]{3,2,1,0:T(4,128)(2,1)}, u32[]{:S(2)}, u32[]{:S(2)}) async-start(bf16[8,112,4,128]{3,2,1,0:T(4,128)(2,1)} %copy.125), calls=%async_computation.1 | async-start | bytes 1835008 | tf_op jit(solution)/shard_map/all_to_all | solution.py:20
  114.6 22.2 %all-to-all-start.2 = ((bf16[64,2,4,128]{3,1,2,0:T(2,128)(2,1)}), bf16[64,2,4,128]{3,1,2,0:T(2,128)(2,1)S(1)}, u32[]{:S(2)}, u32[]{:S(2)}) async-start(bf16[64,2,4,128]{3,1,2,0:T(2,128)(2,1)} %copy.129), calls=%async_computation.2 | async-start | bytes 262144 | tf_op jit(solution)/shard_map/all_to_all | solution.py:124
  136.8 37.4 %all-to-all-start.3 = ((bf16[64,32,128]{2,1,0:T(8,128)(2,1)}), bf16[64,32,128]{2,1,0:T(8,128)(2,1)S(1)}, u32[]{:S(2)}, u32[]{:S(2)}) async-start(bf16[64,32,128]{2,1,0:T(8,128)(2,1)} %bitcast.36), calls=%async_computation.3 | async-start | bytes 1048576 | tf_op jit(solution)/shard_map/all_to_all | solution.py:20
where the time goes:
time: 176 us; the launch traced here: 175 us
  waiting for transfers between devices  106 us (60%)
  starting transfers between devices  34.6 us (20%)
  local copies, waits for them, and re-layouts  17.1 us (10%)
  matrix products  9.69 us (6%)
  other arithmetic  6.77 us (4%)
    all_to_all x1, waiting for transfers between devices, body(): lax.all_to_all(outgoing, 'kv', split_axis=0, concat_axis=0, tiled=True)  49.2 us
    all_to_all x2, waiting for transfers between devices, sum_at_owner(): lax.all_to_all(in_blocks(array, dim, peers), axis, 0, 0, tiled=True)  44.8 us
    all_to_all x1, starting transfers between devices, body(): lax.all_to_all(outgoing, 'kv', split_axis=0, concat_axis=0, tiled=True)  18.7 us
    all_to_all x1, waiting for transfers between devices, body(): lax.all_to_all(summed[:slot_count].reshape(kv_count, CAP, key_share, 2 *...  11.8 us
    all_to_all x2, starting transfers between devices, sum_at_owner(): lax.all_to_all(in_blocks(array, dim, peers), axis, 0, 0, tiled=True)  9.91 us
    all_to_all x1, starting transfers between devices, body(): lax.all_to_all(summed[:slot_count].reshape(kv_count, CAP, key_share, 2 *...  5.95 us
  transfers between devices with their start and end apart: 4, of which 4 were waited for; matrix products, arithmetic and copies ran while one was open for 7% of the time, Pallas kernels for 0%

commit v1 on v0

v1 whole, which is shorter than its diff:
```python
import jax
import jax.numpy as jnp
from jax import lax
from jax.experimental import pallas as pl
from jax.experimental.pallas import tpu as pltpu
from jax.sharding import Mesh
from jax.sharding import PartitionSpec as P

DH = 64
QB = 128
KB = 32
NSEL = 16
CAP = 2

TOK = 896
PER = TOK // QB
OWN = TOK // KB
KV = 64
TP = 8
DIAG = QB // KB
REM = NSEL - DIAG
PIECE = KB // TP
ROWS = NSEL * PIECE
REM_ROWS = REM * PIECE
KEYS = NSEL * KB
SLOTS = KV * CAP * PIECE
NONE = -4096

VMEM = pl.BlockSpec(memory_space=pltpu.VMEM)
SMEM = pl.BlockSpec(memory_space=pltpu.SMEM)


def call(kernel, out_shape, args, scratch=(), name=None):
    specs = [SMEM if a.ndim == 1 and a.dtype == jnp.int32 else VMEM for a in args]
    outs = jax.tree.map(lambda _: VMEM, out_shape)
    return pl.pallas_call(
        kernel, out_shape=out_shape, in_specs=specs, out_specs=outs, scratch_shapes=list(scratch), name=name
    )(*args)


def offer_kernel(place_ref, sel_ref, kv_ref, out_ref, slot_ref):
    me, member = place_ref[0], place_ref[1]
    local = (sel_ref[...] - me * OWN).astype(jnp.float32)
    inside = (local >= 0) & (local < OWN)
    least = jnp.min(jnp.where(inside, local, 1000.0), axis=0, keepdims=True)
    most = jnp.max(jnp.where(inside, local, -1000.0), axis=0, keepdims=True)
    shape = (SLOTS, KV * PER)
    row = lax.broadcasted_iota(jnp.int32, shape, 0)
    lane = lax.broadcasted_iota(jnp.int32, shape, 1)
    first_lane = (row >> 3) * PER
    second = ((row >> 2) & 1) == 1
    choice = jnp.where(second, jnp.broadcast_to(-most, shape), jnp.broadcast_to(least, shape))
    in_row = (lane >= first_lane) & (lane < first_lane + PER)
    slot = jnp.min(jnp.where(in_row, choice, 1000.0), axis=1, keepdims=True)
    rows = lax.broadcasted_iota(jnp.int32, (SLOTS, 1), 0)
    slot = jnp.where(((rows >> 2) & 1) == 1, -slot, slot)
    slot = jnp.where((rows >> 3) == me, 1000.0, slot)
    slot = jnp.where(jnp.abs(slot) < OWN, slot, -1000.0).astype(jnp.int32)
    target = slot * KB + member * PIECE + (rows & (PIECE - 1))
    onehot = lax.broadcasted_iota(jnp.int32, (SLOTS, TOK), 1) == target
    out_ref[...] = jnp.dot(
        onehot.astype(jnp.bfloat16), kv_ref[...], preferred_element_type=jnp.float32
    ).astype(jnp.bfloat16)
    home = (slot * PIECE + (rows & (PIECE - 1))).astype(jnp.float32)
    slot_ref[...] = jnp.broadcast_to(home, (SLOTS, 128)).T[:8]


def pick_kernel(target_ref, fetched_ref, out_ref):
    column = jnp.broadcast_to(target_ref[...], (128, KEYS)).T
    parts = [
        (column == lax.broadcasted_iota(jnp.int32, (KEYS, 128), 1).astype(jnp.float32) + 128.0 * j)
        for j in range(SLOTS // 128)
    ]
    onehot = jnp.concatenate([p.astype(jnp.bfloat16) for p in parts], axis=1)
    rows = jnp.dot(onehot, fetched_ref[...], preferred_element_type=jnp.float32).astype(jnp.bfloat16)
    for t in range(TP):
        out_ref[t] = rows[t * ROWS : t * ROWS + REM_ROWS]


def attention_kernel(bias_ref, remote_ref, own_ref, q_ref, g_ref, log_ref, dq_ref, dkv_ref, kv_ref, sum_ref, mask_ref):
    scale = DH ** (-0.5)
    for p in range(TP):
        kv_ref[p * ROWS : p * ROWS + REM_ROWS] = remote_ref[p]
        kv_ref[p * ROWS + REM_ROWS : (p + 1) * ROWS] = own_ref[p]
    kv = kv_ref[...]
    shape = (KEYS, QB)
    key = lax.broadcasted_iota(jnp.int32, shape, 0)
    query = lax.broadcasted_iota(jnp.int32, shape, 1)
    within = key & (ROWS - 1)
    position = ((within >> 2) - REM) * KB + (key >> 6) * PIECE + (within & (PIECE - 1))
    live = (within < REM_ROWS) | (position <= query)
    bias = jnp.broadcast_to(bias_ref[...], (QB, KEYS)).T
    mask_ref[...] = jnp.where(live, bias, -1e30)
    sum_ref[...] = jnp.zeros_like(sum_ref)
    key_t = kv[:, :DH].T
    keys = kv[:, :DH]
    values = kv[:, DH:]
    zero = jnp.zeros((QB, DH), jnp.bfloat16)

    def pair(s, carry):
        q_pair, g_pair = q_ref[s], g_ref[s]
        log_pair = log_ref[s]
        turned = []
        for h in range(2):
            q = q_pair[:, h * DH : (h + 1) * DH]
            g = g_pair[:, h * DH : (h + 1) * DH]
            contract = (((1,), (1,)), ((), ()))
            scores = lax.dot_general(keys, q, contract, preferred_element_type=jnp.float32)
            dprob = lax.dot_general(values, g, contract, preferred_element_type=jnp.float32)
            prob = jnp.exp(scores * scale + (mask_ref[...] - log_pair[h : h + 1]))
            prob_b = prob.astype(jnp.bfloat16)
            delta = jnp.sum(prob_b.astype(jnp.float32) * dprob, axis=0, keepdims=True)
            dscore_b = (prob * (dprob - delta)).astype(jnp.bfloat16)
            turned.append(jnp.dot(key_t, dscore_b, preferred_element_type=jnp.float32))
            left = jnp.concatenate([dscore_b, prob_b], axis=1)
            right = jnp.concatenate(
                [jnp.concatenate([q, zero], axis=1), jnp.concatenate([zero, g], axis=1)], axis=0
            )
            sum_ref[...] += jnp.dot(left, right, preferred_element_type=jnp.float32)
        dq_ref[s] = (jnp.concatenate(turned, axis=0) * scale).T.astype(jnp.bfloat16)
        return carry

    lax.fori_loop(0, TP, pair, 0)
    lane = lax.broadcasted_iota(jnp.int32, (KEYS, 2 * DH), 1)
    total = sum_ref[...] * jnp.where(lane < DH, scale, 1.0)
    dkv_ref[...] = total.astype(jnp.bfloat16).reshape(TP, ROWS, 2 * DH)


def spread_kernel(target_ref, grads_ref, out_ref):
    row = lax.broadcasted_iota(jnp.int32, (SLOTS, KEYS), 0).astype(jnp.float32)
    onehot = (row == target_ref[...]).astype(jnp.bfloat16)
    out_ref[...] = jnp.dot(onehot, grads_ref[...], preferred_element_type=jnp.float32).astype(jnp.bfloat16)


def home_kernel(slot_ref, returned_ref, grads_ref, out_ref):
    row = lax.broadcasted_iota(jnp.int32, (OWN * PIECE, SLOTS), 0).astype(jnp.float32)
    onehot = (row == slot_ref[0:1]).astype(jnp.bfloat16)
    total = jnp.dot(onehot, returned_ref[...], preferred_element_type=jnp.float32)
    own = [grads_ref[t, REM_ROWS:, :].astype(jnp.float32) for t in range(PER)]
    out_ref[...] = total + jnp.concatenate(own, axis=0)


def weight_kernel(grad_ref, in_ref, out_ref, turned_ref):
    @pl.when(pl.program_id(0) == 0)
    def _():
        for t in range(PER):
            turned_ref[:, t * QB : (t + 1) * QB] = grad_ref[t].T

    term = jnp.dot(turned_ref[...], in_ref[...], preferred_element_type=jnp.float32)
    width = in_ref.shape[1]
    term = term.T.astype(jnp.bfloat16)
    for z in range(width // 128):
        for y in range(4):
            at = z * 128 + y * 32
            out_ref[y, z] = term[at : at + 32]


def weight_term(grads, inputs):
    tile = 256
    return pl.pallas_call(
        weight_kernel,
        grid=(inputs.shape[1] // tile,),
        in_specs=[
            pl.BlockSpec((TP, QB, 2 * DH), lambda i: (0, 0, 0)),
            pl.BlockSpec((TOK, tile), lambda i: (0, i)),
        ],
        out_specs=pl.BlockSpec((4, tile // 128, 32, 2 * DH), lambda i: (0, i, 0, 0)),
        out_shape=jax.ShapeDtypeStruct((4, 16, 32, 2 * DH), jnp.bfloat16),
        scratch_shapes=[pltpu.VMEM((2 * DH, TOK), jnp.bfloat16)],
        name="weight",
    )(grads, inputs)


def swap(array, axis):
    return lax.all_to_all(array, axis, 0, 0, tiled=True)


def padded(array):
    return jnp.concatenate([array.reshape(PER, QB, 2 * DH), jnp.zeros((1, QB, 2 * DH), array.dtype)], axis=0)


def body(queries, keyvals, log_sums, out_grad, inputs, selection):
    kv_axes = ("z", "y")
    me = lax.axis_index(kv_axes)
    member = lax.axis_index("tp")
    bf16 = jnp.bfloat16
    place = jnp.stack([me, member]).astype(jnp.int32)

    offer, slots = call(
        offer_kernel,
        [jax.ShapeDtypeStruct((SLOTS, 2 * DH), bf16), jax.ShapeDtypeStruct((8, SLOTS), jnp.float32)],
        [place, selection.T, keyvals],
        name="offer",
    )
    fetched = swap(offer.reshape(KV, CAP * PIECE, 2 * DH), kv_axes)

    q_all = swap(padded(queries), "tp")
    g_all = swap(padded(out_grad), "tp")
    log_rows = jnp.pad(log_sums.reshape(2, PER, QB).transpose(1, 0, 2), ((0, 1), (0, 0), (0, 0)))
    log_all = swap(log_rows, "tp")

    mine = lax.dynamic_slice(selection, (me * PER, 0), (PER, NSEL))[:, DIAG:]
    flat = mine.reshape(-1)
    owner = flat // OWN
    same = owner[:, None] == owner[None, :]
    least = jnp.min(jnp.where(same, flat[None, :], 1 << 20), axis=1)
    slot = jnp.where(flat != least, PIECE, 0)
    target = jnp.where(flat >= 0, owner * (CAP * PIECE) + slot, NONE).reshape(PER, REM)
    target = jnp.pad(target, ((0, 1), (0, DIAG)), constant_values=NONE)
    live = (target >= 0) | (
        (jnp.arange(NSEL)[None, :] >= REM) & (jnp.arange(TP)[:, None] < PER)
    )
    target = (target[:, :, None] + jnp.arange(PIECE)).reshape(1, KEYS).astype(jnp.float32)
    live = lax.dynamic_index_in_dim(live, member, 0, keepdims=True)
    bias = jnp.where(live, 0.0, -1e30).astype(jnp.float32)
    bias = jnp.broadcast_to(bias[:, None, :, None], (1, TP, NSEL, PIECE)).reshape(1, KEYS)
    own_at = jnp.minimum(member, PER - 1) * QB
    own = lax.dynamic_slice(keyvals, (own_at, 0), (QB, 2 * DH))
    own = own.reshape(DIAG, TP, PIECE, 2 * DH).transpose(1, 0, 2, 3).reshape(TP, DIAG * PIECE, 2 * DH)

    picked = call(
        pick_kernel,
        jax.ShapeDtypeStruct((TP, REM_ROWS, 2 * DH), bf16),
        [target, fetched.reshape(SLOTS, 2 * DH)],
        name="pick",
    )
    remote = swap(picked, "tp")

    dq, dkv = call(
        attention_kernel,
        [jax.ShapeDtypeStruct((TP, QB, 2 * DH), bf16), jax.ShapeDtypeStruct((TP, ROWS, 2 * DH), bf16)],
        [bias, remote, own, q_all, g_all, log_all],
        scratch=[
            pltpu.VMEM((KEYS, 2 * DH), bf16),
            pltpu.VMEM((KEYS, 2 * DH), jnp.float32),
            pltpu.VMEM((KEYS, QB), jnp.float32),
        ],
        name="attention",
    )
    dq_mine = swap(dq, "tp")
    query_grad = dq_mine[:PER].reshape(TOK, 2 * DH)

    entry_grads = swap(dkv, "tp")
    term = weight_term(dq_mine, inputs)
    by_y = swap(term, "y")
    spread = call(
        spread_kernel,
        jax.ShapeDtypeStruct((SLOTS, 2 * DH), bf16),
        [target, entry_grads.reshape(KEYS, 2 * DH)],
        name="spread",
    )
    returned = swap(spread.reshape(KV, CAP * PIECE, 2 * DH), kv_axes)
    keyval_grad = call(
        home_kernel,
        jax.ShapeDtypeStruct((OWN * PIECE, 2 * DH), jnp.float32),
        [slots, returned.reshape(SLOTS, 2 * DH), entry_grads],
        name="home",
    ).reshape(OWN, PIECE, 2 * DH)
    by_y = jnp.sum(by_y.astype(jnp.float32), axis=0).astype(bf16)
    by_z = swap(by_y, "z")
    weight_grad = jnp.sum(by_z.astype(jnp.float32), axis=0)
    return query_grad, keyval_grad, weight_grad


def solution(mesh):
    split = Mesh(mesh.devices.reshape(16, 4, TP), ("z", "y", "tp"))
    kv = ("z", "y")
    return jax.shard_map(
        body,
        mesh=split,
        in_specs=(P(kv, "tp"), P(kv, None), P("tp", kv), P(kv, "tp"), P(kv, None), P()),
        out_specs=(P(kv, "tp"), P(kv, "tp", None), P(kv, "tp")),
        check_vma=False,
    )
```

time: 176 us -> 166 us (0.943)
  the two profiles are of different devices: /device:TPU:8 before, /device:TPU:2 now
where the time goes in v1:
time: 166 us; the launch traced here: 164 us
  waiting for transfers between devices  60.7 us (37%)
  starting transfers between devices  54.3 us (33%)
  Pallas kernels  24.7 us (15%)
  blocking collectives  11.5 us (7%)
  local copies, waits for them, and re-layouts  9.87 us (6%)
  other arithmetic  2.42 us (1%)
    all_to_all x9, waiting for transfers between devices, swap(): return lax.all_to_all(array, axis, 0, 0, tiled=True)  60.7 us
    all_to_all x9, starting transfers between devices, swap(): return lax.all_to_all(array, axis, 0, 0, tiled=True)  54.3 us
    pallas_call x5, Pallas kernels, call(): pl.pallas_call(kernel, out_shape=out_shape, in_specs=specs, out_specs=out...  17.7 us
    all_to_all x1, blocking collectives, swap(): return lax.all_to_all(array, axis, 0, 0, tiled=True)  11.5 us
    pallas_call x1, Pallas kernels, weight_term(): pl.pallas_call(weight_kernel, grid=(inputs.shape[1] // tile,), in_specs=[...  6.93 us
  transfers between devices with their start and end apart: 9, of which 8 were waited for; matrix products, arithmetic and copies ran while one was open for 6% of the time, Pallas kernels for 9%

profile of v1, /device:TPU:2, one launch (start us, length us, event | category | flops | bytes accessed | tf_op | source)
XLA Modules:
  0.0 164.2 jit_solution(3643410578171265929)
XLA Ops:
  1.9 9.1 %all-to-all-start.4 = ((f32[8,2,128]{2,1,0:T(2,128)}), f32[8,2,128]{2,1,0:T(2,128)S(1)}, u32[]{:S(2)}, u32[]{:S(2)}) async-start(f32[8,2,128]{2,1,0:T(2,128)} %pad.11), calls=%async_computation.4 | async-start | bytes 16384 | tf_op jit(solution)/shard_map/all_to_all | solution.py:175
  14.9 4.8 %all-to-all-start.2 = ((bf16[8,128,128]{2,1,0:T(8,128)(2,1)}), bf16[8,128,128]{2,1,0:T(8,128)(2,1)S(1)}, u32[]{:S(2)}, u32[]{:S(2)}) async-start(bf16[8,128,128]{2,1,0:T(8,128)(2,1)} %concatenate.6), calls=%async_computation.2 | async-start | bytes 524288 | tf_op jit(solution)/shard_map/all_to_all | solution.py:175
  20.7 2.4 %offer.1 = (bf16[512,128]{1,0:T(8,128)(2,1)}, f32[8,512]{1,0:T(8,128)}) custom-call(s32[2]{0:T(128)} %pad_add_fusion.place_ref, s32[16,448]{1,0:T(8,128)} %bitcast.32, bf16[896,128]{1,0:T(8,128)(2,1)} %kv_ref.1), custom_call_target="tpu_custom_call" | custom-call | tf_op jit(solution)/shard_map/offer/pallas_call | solution.py:36
  23.1 2.7 %all-to-all-done.2.q_ref = bf16[8,128,128]{2,1,0:T(8,128)(2,1)S(1)} async-done(((bf16[8,128,128]{2,1,0:T(8,128)(2,1)}), bf16[8,128,128]{2,1,0:T(8,128)(2,1)S(1)}, u32[]{:S(2)}, u32[]{:S(2)}) %all-to-all-start.2) | async-done | bytes 262176 | tf_op jit(solution)/shard_map/all_to_all | solution.py:175
  25.8 14.4 %all-to-all-start = ((bf16[64,8,128]{2,1,0:T(8,128)(2,1)}), bf16[64,8,128]{2,1,0:T(8,128)(2,1)S(1)}, u32[]{:S(2)}, u32[]{:S(2)}) async-start(bf16[64,8,128]{2,1,0:T(8,128)(2,1)} %bitcast.28), calls=%async_computation | async-start | bytes 262144 | tf_op jit(solution)/shard_map/all_to_all | solution.py:175
  40.3 1.7 %concatenate.7 = bf16[8,128,128]{2,1,0:T(8,128)(2,1)} pad(bf16[7,128,128]{2,1,0:T(8,128)(2,1)} %bitcast.26, bf16[]{:T(256)} %constant.62.clone.1), padding=0_1x0_0x0_0 | pad | bytes 491522 | tf_op jit(solution)/shard_map/concatenate | solution.py:179
  42.8 14.7 %all-to-all-done = bf16[64,8,128]{2,1,0:T(8,128)(2,1)S(1)} async-done(((bf16[64,8,128]{2,1,0:T(8,128)(2,1)}), bf16[64,8,128]{2,1,0:T(8,128)(2,1)S(1)}, u32[]{:S(2)}, u32[]{:S(2)}) %all-to-all-start) | async-done | bytes 131104 | tf_op jit(solution)/shard_map/all_to_all | solution.py:175
  57.5 4.8 %all-to-all-start.3 = ((bf16[8,128,128]{2,1,0:T(8,128)(2,1)}), bf16[8,128,128]{2,1,0:T(8,128)(2,1)S(1)}, u32[]{:S(2)}, u32[]{:S(2)}) async-start(bf16[8,128,128]{2,1,0:T(8,128)(2,1)} %concatenate.7), calls=%async_computation.3 | async-start | bytes 524288 | tf_op jit(solution)/shard_map/all_to_all | solution.py:175
  63.6 1.9 %pick.1 = bf16[8,48,128]{2,1,0:T(8,128)(2,1)} custom-call(f32[1,512]{1,0:T(1,128)} %convert_element_type.13.target_ref, bf16[512,128]{1,0:T(8,128)(2,1)} %bitcast.22), custom_call_target="tpu_custom_call" | custom-call | tf_op jit(solution)/shard_map/pick/pallas_call | solution.py:36
  65.5 2.8 %all-to-all-done.3.g_ref = bf16[8,128,128]{2,1,0:T(8,128)(2,1)S(1)} async-done(((bf16[8,128,128]{2,1,0:T(8,128)(2,1)}), bf16[8,128,128]{2,1,0:T(8,128)(2,1)S(1)}, u32[]{:S(2)}, u32[]{:S(2)}) %all-to-all-start.3) | async-done | bytes 262176 | tf_op jit(solution)/shard_map/all_to_all | solution.py:175
  68.3 4.7 %all-to-all-start.1 = ((bf16[8,48,128]{2,1,0:T(8,128)(2,1)}), bf16[8,48,128]{2,1,0:T(8,128)(2,1)S(1)}, u32[]{:S(2)}, u32[]{:S(2)}) async-start(bf16[8,48,128]{2,1,0:T(8,128)(2,1)} %pick.1), calls=%async_computation.1 | async-start | bytes 196608 | tf_op jit(solution)/shard_map/all_to_all | solution.py:175
  73.8 3.6 %all-to-all-done.1.remote_ref = bf16[8,48,128]{2,1,0:T(8,128)(2,1)S(1)} async-done(((bf16[8,48,128]{2,1,0:T(8,128)(2,1)}), bf16[8,48,128]{2,1,0:T(8,128)(2,1)S(1)}, u32[]{:S(2)}, u32[]{:S(2)}) %all-to-all-start.1) | async-done | bytes 98336 | tf_op jit(solution)/shard_map/all_to_all | solution.py:175
  78.0 9.8 %attention.1 = (bf16[8,128,128]{2,1,0:T(8,128)(2,1)}, bf16[8,64,128]{2,1,0:T(8,128)(2,1)}) custom-call(f32[1,512]{1,0:T(1,128)} %broadcast_in_dim.54.bias_ref, bf16[8,48,128]{2,1,0:T(8,128)(2,1)} %copy-done.6, bf16[8,16,128]{2,1,0:T(8,128)(2,1)} %bitcast.30, bf16[8,128,128]{2,1,0:T(8,128)(2,1)} %copy-done.2, bf16[8,128,128]{2,1,0:T(8,128)(2,1)} %copy-done.3, ...), custom_call_target="tpu_custom_call" | custom-call | tf_op jit(solution)/shard_map/attention/pallas_call | solution.py:36
  87.9 11.5 %all_to_all.50.grad_ref = bf16[8,128,128]{2,1,0:T(8,128)(2,1)} all-to-all(bf16[8,128,128]{2,1,0:T(8,128)(2,1)} %get-tuple-element.8), channel_id=1, replica_groups=mesh['z'=16,'y'=4,'tp'=8] {'tp'}, dimensions={0} | all-to-all | bytes 524288 | tf_op jit(solution)/shard_map/all_to_all | solution.py:175
  99.4 4.9 %all-to-all-start.6 = ((bf16[8,64,128]{2,1,0:T(8,128)(2,1)}), bf16[8,64,128]{2,1,0:T(8,128)(2,1)S(1)}, u32[]{:S(2)}, u32[]{:S(2)}) async-start(bf16[8,64,128]{2,1,0:T(8,128)(2,1)} %get-tuple-element.10), calls=%async_computation.6 | async-start | bytes 262144 | tf_op jit(solution)/shard_map/all_to_all | solution.py:175
  104.3 6.9 %weight.1 = bf16[4,16,32,128]{3,2,1,0:T(8,128)(2,1)} custom-call(bf16[8,128,128]{2,1,0:T(8,128)(2,1)} %all_to_all.50.grad_ref, bf16[896,2048]{1,0:T(8,128)(2,1)} %in_ref.1), custom_call_target="tpu_custom_call" | custom-call | tf_op jit(solution)/shard_map/weight/pallas_call | solution.py:160
  111.2 3.5 %all-to-all-start.8 = ((bf16[4,16,32,128]{3,2,1,0:T(8,128)(2,1)}), bf16[4,16,32,128]{3,2,1,0:T(8,128)(2,1)S(1)}, u32[]{:S(2)}, u32[]{:S(2)}) async-start(bf16[4,16,32,128]{3,2,1,0:T(8,128)(2,1)} %weight.1), calls=%async_computation.8 | async-start | bytes 1048576 | tf_op jit(solution)/shard_map/all_to_all | solution.py:175
  114.7 1.9 %spread.1 = bf16[512,128]{1,0:T(8,128)(2,1)} custom-call(f32[1,512]{1,0:T(1,128)} %convert_element_type.13.target_ref, bf16[512,128]{1,0:T(8,128)(2,1)} %bitcast.21), custom_call_target="tpu_custom_call" | custom-call | tf_op jit(solution)/shard_map/spread/pallas_call | solution.py:36
  116.5 8.1 %all-to-all-done.8 = bf16[4,16,32,128]{3,2,1,0:T(8,128)(2,1)S(1)} async-done(((bf16[4,16,32,128]{3,2,1,0:T(8,128)(2,1)}), bf16[4,16,32,128]{3,2,1,0:T(8,128)(2,1)S(1)}, u32[]{:S(2)}, u32[]{:S(2)}) %all-to-all-start.8) | async-done | bytes 524320 | tf_op jit(solution)/shard_map/all_to_all | solution.py:175
  124.7 4.6 %all-to-all-start.7 = ((bf16[64,8,128]{2,1,0:T(8,128)(2,1)}), bf16[64,8,128]{2,1,0:T(8,128)(2,1)S(1)}, u32[]{:S(2)}, u32[]{:S(2)}) async-start(bf16[64,8,128]{2,1,0:T(8,128)(2,1)} %bitcast.23), calls=%async_computation.7 | async-start | bytes 262144 | tf_op jit(solution)/shard_map/all_to_all | solution.py:175
  130.1 16.8 %all-to-all-done.7 = bf16[64,8,128]{2,1,0:T(8,128)(2,1)S(1)} async-done(((bf16[64,8,128]{2,1,0:T(8,128)(2,1)}), bf16[64,8,128]{2,1,0:T(8,128)(2,1)S(1)}, u32[]{:S(2)}, u32[]{:S(2)}) %all-to-all-start.7) | async-done | bytes 131104 | tf_op jit(solution)/shard_map/all_to_all | solution.py:175
  146.8 3.5 %all-to-all-start.9 = ((bf16[16,32,128]{2,1,0:T(8,128)(2,1)}), bf16[16,32,128]{2,1,0:T(8,128)(2,1)S(1)}, u32[]{:S(2)}, u32[]{:S(2)}) async-start(bf16[16,32,128]{2,1,0:T(8,128)(2,1)} %reduce_sum.21), calls=%async_computation.9 | async-start | bytes 262144 | tf_op jit(solution)/shard_map/all_to_all | solution.py:175
  151.1 1.8 %home.1 = f32[112,128]{1,0:T(8,128)} custom-call(f32[8,512]{1,0:T(8,128)} %get-tuple-element.9.slot_ref, bf16[512,128]{1,0:T(8,128)(2,1)} %bitcast.24, bf16[8,64,128]{2,1,0:T(8,128)(2,1)} %copy-done.1), custom_call_target="tpu_custom_call" | custom-call | tf_op jit(solution)/shard_map/home/pallas_call | solution.py:36
  152.8 10.7 %all-to-all-done.9 = bf16[16,32,128]{2,1,0:T(8,128)(2,1)S(1)} async-done(((bf16[16,32,128]{2,1,0:T(8,128)(2,1)}), bf16[16,32,128]{2,1,0:T(8,128)(2,1)S(1)}, u32[]{:S(2)}, u32[]{:S(2)}) %all-to-all-start.9) | async-done | bytes 131104 | tf_op jit(solution)/shard_map/all_to_all | solution.py:175
  (42 shorter events, 11.9 us)
Async XLA Ops:
  1.9 13.0 %all-to-all-start.4 = ((f32[8,2,128]{2,1,0:T(2,128)}), f32[8,2,128]{2,1,0:T(2,128)S(1)}, u32[]{:S(2)}, u32[]{:S(2)}) async-start(f32[8,2,128]{2,1,0:T(2,128)} %pad.11), calls=%async_computation.4 | async-start | bytes 16384 | tf_op jit(solution)/shard_map/all_to_all | solution.py:175
  14.9 62.5 %copy-start.7 = (f32[8,2,128]{2,1,0:T(2,128)}, f32[8,2,128]{2,1,0:T(2,128)S(1)}, u32[]{:S(2)}) copy-start(f32[8,2,128]{2,1,0:T(2,128)S(1)} %all-to-all-done.4.log_ref) | copy-start | bytes 24580
  14.9 10.8 %all-to-all-start.2 = ((bf16[8,128,128]{2,1,0:T(8,128)(2,1)}), bf16[8,128,128]{2,1,0:T(8,128)(2,1)S(1)}, u32[]{:S(2)}, u32[]{:S(2)}) async-start(bf16[8,128,128]{2,1,0:T(8,128)(2,1)} %concatenate.6), calls=%async_computation.2 | async-start | bytes 524288 | tf_op jit(solution)/shard_map/all_to_all | solution.py:175
  25.8 51.6 %copy-start.2 = (bf16[8,128,128]{2,1,0:T(8,128)(2,1)}, bf16[8,128,128]{2,1,0:T(8,128)(2,1)S(1)}, u32[]{:S(2)}) copy-start(bf16[8,128,128]{2,1,0:T(8,128)(2,1)S(1)} %all-to-all-done.2.q_ref) | copy-start | bytes 786436
  25.8 31.7 %all-to-all-start = ((bf16[64,8,128]{2,1,0:T(8,128)(2,1)}), bf16[64,8,128]{2,1,0:T(8,128)(2,1)S(1)}, u32[]{:S(2)}, u32[]{:S(2)}) async-start(bf16[64,8,128]{2,1,0:T(8,128)(2,1)} %bitcast.28), calls=%async_computation | async-start | bytes 262144 | tf_op jit(solution)/shard_map/all_to_all | solution.py:175
  57.5 6.2 %copy-start.4 = (bf16[64,8,128]{2,1,0:T(8,128)(2,1)}, bf16[64,8,128]{2,1,0:T(8,128)(2,1)S(1)}, u32[]{:S(2)}) copy-start(bf16[64,8,128]{2,1,0:T(8,128)(2,1)S(1)} %all-to-all-done) | copy-start | bytes 393220
  57.5 10.8 %all-to-all-start.3 = ((bf16[8,128,128]{2,1,0:T(8,128)(2,1)}), bf16[8,128,128]{2,1,0:T(8,128)(2,1)S(1)}, u32[]{:S(2)}, u32[]{:S(2)}) async-start(bf16[8,128,128]{2,1,0:T(8,128)(2,1)} %concatenate.7), calls=%async_computation.3 | async-start | bytes 524288 | tf_op jit(solution)/shard_map/all_to_all | solution.py:175
  68.3 9.1 %copy-start.3 = (bf16[8,128,128]{2,1,0:T(8,128)(2,1)}, bf16[8,128,128]{2,1,0:T(8,128)(2,1)S(1)}, u32[]{:S(2)}) copy-start(bf16[8,128,128]{2,1,0:T(8,128)(2,1)S(1)} %all-to-all-done.3.g_ref) | copy-start | bytes 786436
  68.3 9.1 %all-to-all-start.1 = ((bf16[8,48,128]{2,1,0:T(8,128)(2,1)}), bf16[8,48,128]{2,1,0:T(8,128)(2,1)S(1)}, u32[]{:S(2)}, u32[]{:S(2)}) async-start(bf16[8,48,128]{2,1,0:T(8,128)(2,1)} %pick.1), calls=%async_computation.1 | async-start | bytes 196608 | tf_op jit(solution)/shard_map/all_to_all | solution.py:175
  77.4 0.6 copy-start.6
  99.4 51.0 %copy-start = (bf16[8,128,128]{2,1,0:T(8,128)(2,1)S(1)}, bf16[8,128,128]{2,1,0:T(8,128)(2,1)}, u32[]{:S(2)}) copy-start(bf16[8,128,128]{2,1,0:T(8,128)(2,1)} %all_to_all.50.grad_ref) | copy-start | bytes 786436
  99.4 11.8 %all-to-all-start.6 = ((bf16[8,64,128]{2,1,0:T(8,128)(2,1)}), bf16[8,64,128]{2,1,0:T(8,128)(2,1)S(1)}, u32[]{:S(2)}, u32[]{:S(2)}) async-start(bf16[8,64,128]{2,1,0:T(8,128)(2,1)} %get-tuple-element.10), calls=%async_computation.6 | async-start | bytes 262144 | tf_op jit(solution)/shard_map/all_to_all | solution.py:175
  111.2 3.5 %copy-start.1 = (bf16[8,64,128]{2,1,0:T(8,128)(2,1)}, bf16[8,64,128]{2,1,0:T(8,128)(2,1)S(1)}, u32[]{:S(2)}) copy-start(bf16[8,64,128]{2,1,0:T(8,128)(2,1)S(1)} %all-to-all-done.6.grads_ref) | copy-start | bytes 393220
  111.2 13.5 %all-to-all-start.8 = ((bf16[4,16,32,128]{3,2,1,0:T(8,128)(2,1)}), bf16[4,16,32,128]{3,2,1,0:T(8,128)(2,1)S(1)}, u32[]{:S(2)}, u32[]{:S(2)}) async-start(bf16[4,16,32,128]{3,2,1,0:T(8,128)(2,1)} %weight.1), calls=%async_computation.8 | async-start | bytes 1048576 | tf_op jit(solution)/shard_map/all_to_all | solution.py:175
  124.7 22.1 %all-to-all-start.7 = ((bf16[64,8,128]{2,1,0:T(8,128)(2,1)}), bf16[64,8,128]{2,1,0:T(8,128)(2,1)S(1)}, u32[]{:S(2)}, u32[]{:S(2)}) async-start(bf16[64,8,128]{2,1,0:T(8,128)(2,1)} %bitcast.23), calls=%async_computation.7 | async-start | bytes 262144 | tf_op jit(solution)/shard_map/all_to_all | solution.py:175
  146.8 4.2 %copy-start.5 = (bf16[64,8,128]{2,1,0:T(8,128)(2,1)}, bf16[64,8,128]{2,1,0:T(8,128)(2,1)S(1)}, u32[]{:S(2)}) copy-start(bf16[64,8,128]{2,1,0:T(8,128)(2,1)S(1)} %all-to-all-done.7) | copy-start | bytes 393220
  146.8 16.7 %all-to-all-start.9 = ((bf16[16,32,128]{2,1,0:T(8,128)(2,1)}), bf16[16,32,128]{2,1,0:T(8,128)(2,1)S(1)}, u32[]{:S(2)}, u32[]{:S(2)}) async-start(bf16[16,32,128]{2,1,0:T(8,128)(2,1)} %reduce_sum.21), calls=%async_computation.9 | async-start | bytes 262144 | tf_op jit(solution)/shard_map/all_to_all | solution.py:175

commit v2 on v1

v2 whole, which is shorter than its diff:
```python
import jax
import jax.numpy as jnp
from jax import lax
from jax.experimental import pallas as pl
from jax.experimental.pallas import tpu as pltpu
from jax.sharding import Mesh
from jax.sharding import PartitionSpec as P

DH = 64
QB = 128
KB = 32
NSEL = 16
CAP = 2

TOK = 896
PER = TOK // QB
OWN = TOK // KB
KV = 64
TP = 8
DIAG = QB // KB
REM = NSEL - DIAG
PIECE = KB // TP
ROWS = NSEL * PIECE
REM_ROWS = REM * PIECE
KEYS = NSEL * KB
SLOTS = KV * CAP * PIECE
NONE = -4096
Q_AT = REM_ROWS
G_AT = Q_AT + QB
LOG_AT = G_AT + QB
SEND = LOG_AT + 16
SLOT_ROWS = CAP * PIECE
W_ROWS = 32

VMEM = pl.BlockSpec(memory_space=pltpu.VMEM)
GRANT = 12 << 20


def call(kernel, out_shape, args, scratch=(), name=None):
    return pl.pallas_call(
        kernel,
        out_shape=out_shape,
        in_specs=[VMEM for _ in args],
        out_specs=jax.tree.map(lambda _: VMEM, out_shape),
        scratch_shapes=list(scratch),
        compiler_params=pltpu.CompilerParams(vmem_limit_bytes=GRANT),
        name=name,
    )(*args)


def kv_index():
    return lax.axis_index("z") * 4 + lax.axis_index("y")


def offer_kernel(sel_ref, kv_ref, out_ref, slot_ref):
    me, member = kv_index(), lax.axis_index("tp")
    local = (sel_ref[...] - me * OWN).astype(jnp.float32)
    inside = (local >= 0) & (local < OWN)
    least = jnp.min(jnp.where(inside, local, 1000.0), axis=0, keepdims=True)
    most = jnp.max(jnp.where(inside, local, -1000.0), axis=0, keepdims=True)
    shape = (SLOTS, KV * PER)
    row = lax.broadcasted_iota(jnp.int32, shape, 0)
    lane = lax.broadcasted_iota(jnp.int32, shape, 1)
    first_lane = (row >> 3) * PER
    second = ((row >> 2) & 1) == 1
    choice = jnp.where(second, jnp.broadcast_to(-most, shape), jnp.broadcast_to(least, shape))
    in_row = (lane >= first_lane) & (lane < first_lane + PER)
    slot = jnp.min(jnp.where(in_row, choice, 1000.0), axis=1, keepdims=True)
    rows = lax.broadcasted_iota(jnp.int32, (SLOTS, 1), 0)
    slot = jnp.where(((rows >> 2) & 1) == 1, -slot, slot)
    slot = jnp.where((rows >> 3) == me, 1000.0, slot)
    slot = jnp.where(jnp.abs(slot) < OWN, slot, -1000.0).astype(jnp.int32)
    target = slot * KB + member * PIECE + (rows & (PIECE - 1))
    onehot = lax.broadcasted_iota(jnp.int32, (SLOTS, TOK), 1) == target
    out_ref[...] = jnp.dot(
        onehot.astype(jnp.bfloat16), kv_ref[...], preferred_element_type=jnp.float32
    ).astype(jnp.bfloat16)
    home = (slot * PIECE + (rows & (PIECE - 1))).astype(jnp.float32)
    slot_ref[...] = jnp.broadcast_to(home, (SLOTS, 128)).T[:8]


def pick_kernel(target_ref, fetched_ref, q_ref, g_ref, log_ref, out_ref):
    column = jnp.broadcast_to(target_ref[...], (128, KEYS)).T
    parts = [
        (column == lax.broadcasted_iota(jnp.int32, (KEYS, 128), 1).astype(jnp.float32) + 128.0 * j)
        for j in range(SLOTS // 128)
    ]
    onehot = jnp.concatenate([p.astype(jnp.bfloat16) for p in parts], axis=1)
    rows = jnp.dot(onehot, fetched_ref[...], preferred_element_type=jnp.float32).astype(jnp.bfloat16)
    for t in range(TP):
        out_ref[t, :Q_AT] = rows[t * ROWS : t * ROWS + REM_ROWS]
    for t in range(PER):
        at = t * QB
        out_ref[t, Q_AT:G_AT] = q_ref[at : at + QB]
        out_ref[t, G_AT:LOG_AT] = g_ref[at : at + QB]
        rest = log_ref[:, at : at + QB]
        terms = []
        for _ in range(3):
            term = rest.astype(jnp.bfloat16).astype(jnp.float32)
            terms.append(term)
            rest = rest - term
        terms.append(jnp.zeros((10, QB), jnp.float32))
        out_ref[t, LOG_AT:] = jnp.concatenate(terms, axis=0).astype(jnp.bfloat16)
    out_ref[PER, Q_AT:] = jnp.zeros((SEND - Q_AT, 2 * DH), jnp.bfloat16)


def attention_kernel(bias_ref, own_ref, in_ref, out_ref, kv_ref, sum_ref, mask_ref):
    scale = DH ** (-0.5)
    for p in range(TP):
        kv_ref[p * ROWS : p * ROWS + REM_ROWS] = in_ref[p, :Q_AT]
        kv_ref[p * ROWS + REM_ROWS : (p + 1) * ROWS] = own_ref[p]
    kv = kv_ref[...]
    shape = (KEYS, QB)
    key = lax.broadcasted_iota(jnp.int32, shape, 0)
    query = lax.broadcasted_iota(jnp.int32, shape, 1)
    within = key & (ROWS - 1)
    position = ((within >> 2) - REM) * KB + (key >> 6) * PIECE + (within & (PIECE - 1))
    live = (within < REM_ROWS) | (position <= query)
    bias = jnp.broadcast_to(bias_ref[...], (QB, KEYS)).T
    mask_ref[...] = jnp.where(live, bias, -1e30)
    sum_ref[...] = jnp.zeros_like(sum_ref)
    key_t = kv[:, :DH].T
    keys = kv[:, :DH]
    values = kv[:, DH:]
    zero = jnp.zeros((QB, DH), jnp.bfloat16)

    def pair(s, carry):
        q_pair, g_pair = in_ref[s, Q_AT:G_AT], in_ref[s, G_AT:LOG_AT]
        terms = in_ref[s, LOG_AT:].astype(jnp.float32)
        log_pair = (terms[0:2] + terms[2:4]) + terms[4:6]
        turned = []
        for h in range(2):
            q = q_pair[:, h * DH : (h + 1) * DH]
            g = g_pair[:, h * DH : (h + 1) * DH]
            contract = (((1,), (1,)), ((), ()))
            scores = lax.dot_general(keys, q, contract, preferred_element_type=jnp.float32)
            dprob = lax.dot_general(values, g, contract, preferred_element_type=jnp.float32)
            prob = jnp.exp(scores * scale + (mask_ref[...] - log_pair[h : h + 1]))
            prob_b = prob.astype(jnp.bfloat16)
            delta = jnp.sum(prob_b.astype(jnp.float32) * dprob, axis=0, keepdims=True)
            dscore_b = (prob * (dprob - delta)).astype(jnp.bfloat16)
            turned.append(jnp.dot(key_t, dscore_b, preferred_element_type=jnp.float32))
            left = jnp.concatenate([dscore_b, prob_b], axis=1)
            right = jnp.concatenate(
                [jnp.concatenate([q, zero], axis=1), jnp.concatenate([zero, g], axis=1)], axis=0
            )
            sum_ref[...] += jnp.dot(left, right, preferred_element_type=jnp.float32)
        out_ref[s, :QB] = (jnp.concatenate(turned, axis=0) * scale).T.astype(jnp.bfloat16)
        return carry

    lax.fori_loop(0, TP, pair, 0)
    lane = lax.broadcasted_iota(jnp.int32, (KEYS, 2 * DH), 1)
    total = sum_ref[...] * jnp.where(lane < DH, scale, 1.0)
    out_ref[:, QB:] = total.astype(jnp.bfloat16).reshape(TP, ROWS, 2 * DH)


def weight_kernel(target_ref, grad_ref, in_ref, out_ref, turned_ref):
    step = pl.program_id(0)

    @pl.when(step == 0)
    def _():
        for t in range(PER):
            turned_ref[:, t * QB : (t + 1) * QB] = grad_ref[t, :QB].T

    term = jnp.dot(turned_ref[...], in_ref[...], preferred_element_type=jnp.float32)
    term = term.T.astype(jnp.bfloat16)
    shape = (8 * SLOT_ROWS, KEYS)
    row = lax.broadcasted_iota(jnp.int32, shape, 0)
    kv = (step * 2 + ((row >> 3) & 1)) * 4 + (row >> 4)
    slot = kv * SLOT_ROWS + (row & (SLOT_ROWS - 1))
    onehot = (slot.astype(jnp.float32) == target_ref[...]).astype(jnp.bfloat16)
    entries = jnp.concatenate([grad_ref[t, QB:] for t in range(TP)], axis=0)
    spread = jnp.dot(onehot, entries, preferred_element_type=jnp.float32).astype(jnp.bfloat16)
    for y in range(4):
        for z in range(2):
            at = z * 128 + y * W_ROWS
            out_ref[y, z, :W_ROWS] = term[at : at + W_ROWS]
            at = (y * 2 + z) * SLOT_ROWS
            out_ref[y, z, W_ROWS:] = spread[at : at + SLOT_ROWS]


def weight_term(target, grads, inputs):
    tile = 256
    rows = W_ROWS + SLOT_ROWS
    return pl.pallas_call(
        weight_kernel,
        grid=(inputs.shape[1] // tile,),
        in_specs=[
            pl.BlockSpec((1, KEYS), lambda i: (0, 0)),
            pl.BlockSpec((TP, QB + ROWS, 2 * DH), lambda i: (0, 0, 0)),
            pl.BlockSpec((TOK, tile), lambda i: (0, i)),
        ],
        out_specs=pl.BlockSpec((4, tile // 128, rows, 2 * DH), lambda i: (0, i, 0, 0)),
        out_shape=jax.ShapeDtypeStruct((4, 16, rows, 2 * DH), jnp.bfloat16),
        scratch_shapes=[pltpu.VMEM((2 * DH, TOK), jnp.bfloat16)],
        compiler_params=pltpu.CompilerParams(vmem_limit_bytes=GRANT),
        name="weight",
    )(target, grads, inputs)


def regroup_kernel(in_ref, out_ref):
    for z in range(16):
        term = in_ref[0, z, :W_ROWS].astype(jnp.float32)
        for y in range(1, 4):
            term = term + in_ref[y, z, :W_ROWS].astype(jnp.float32)
        out_ref[z, :W_ROWS] = term.astype(jnp.bfloat16)
        for y in range(4):
            at = W_ROWS + y * SLOT_ROWS
            out_ref[z, at : at + SLOT_ROWS] = in_ref[y, z, W_ROWS:]


def home_kernel(slot_ref, returned_ref, grads_ref, kv_grad_ref, weight_ref):
    term = returned_ref[0, :W_ROWS].astype(jnp.float32)
    for z in range(1, 16):
        term = term + returned_ref[z, :W_ROWS].astype(jnp.float32)
    weight_ref[...] = term
    row = lax.broadcasted_iota(jnp.int32, (OWN * PIECE, SLOTS), 0).astype(jnp.float32)
    onehot = (row == slot_ref[0:1]).astype(jnp.bfloat16)
    slots = jnp.concatenate([returned_ref[z, W_ROWS:] for z in range(16)], axis=0)
    total = jnp.dot(onehot, slots, preferred_element_type=jnp.float32)
    own = [grads_ref[t, QB + REM_ROWS :, :].astype(jnp.float32) for t in range(PER)]
    kv_grad_ref[...] = total + jnp.concatenate(own, axis=0)


def swap(array, axis):
    return lax.all_to_all(array, axis, 0, 0, tiled=True)


def body(queries, keyvals, log_sums, out_grad, inputs, selection):
    kv_axes = ("z", "y")
    me = lax.axis_index(kv_axes)
    member = lax.axis_index("tp")
    bf16 = jnp.bfloat16

    offer, slots = call(
        offer_kernel,
        [jax.ShapeDtypeStruct((SLOTS, 2 * DH), bf16), jax.ShapeDtypeStruct((8, SLOTS), jnp.float32)],
        [selection.T, keyvals],
        name="offer",
    )
    fetched = swap(offer.reshape(KV, SLOT_ROWS, 2 * DH), kv_axes)

    mine = lax.dynamic_slice(selection, (me * PER, 0), (PER, NSEL))[:, DIAG:]
    flat = mine.reshape(-1)
    owner = flat // OWN
    same = owner[:, None] == owner[None, :]
    least = jnp.min(jnp.where(same, flat[None, :], 1 << 20), axis=1)
    slot = jnp.where(flat != least, PIECE, 0)
    target = jnp.where(flat >= 0, owner * SLOT_ROWS + slot, NONE).reshape(PER, REM)
    target = jnp.pad(target, ((0, 1), (0, DIAG)), constant_values=NONE)
    live = (target >= 0) | (
        (jnp.arange(NSEL)[None, :] >= REM) & (jnp.arange(TP)[:, None] < PER)
    )
    target = (target[:, :, None] + jnp.arange(PIECE)).reshape(1, KEYS).astype(jnp.float32)
    live = lax.dynamic_index_in_dim(live, member, 0, keepdims=True)
    bias = jnp.where(live, 0.0, -1e30).astype(jnp.float32)
    bias = jnp.broadcast_to(bias[:, None, :, None], (1, TP, NSEL, PIECE)).reshape(1, KEYS)
    own_at = jnp.minimum(member, PER - 1) * QB
    own = lax.dynamic_slice(keyvals, (own_at, 0), (QB, 2 * DH))
    own = own.reshape(DIAG, TP, PIECE, 2 * DH).transpose(1, 0, 2, 3).reshape(TP, DIAG * PIECE, 2 * DH)

    picked = call(
        pick_kernel,
        jax.ShapeDtypeStruct((TP, SEND, 2 * DH), bf16),
        [target, fetched.reshape(SLOTS, 2 * DH), queries, out_grad, log_sums],
        name="pick",
    )
    given = swap(picked, "tp")
    grads = call(
        attention_kernel,
        jax.ShapeDtypeStruct((TP, QB + ROWS, 2 * DH), bf16),
        [bias, own, given],
        scratch=[
            pltpu.VMEM((KEYS, 2 * DH), bf16),
            pltpu.VMEM((KEYS, 2 * DH), jnp.float32),
            pltpu.VMEM((KEYS, QB), jnp.float32),
        ],
        name="attention",
    )
    grads = swap(grads, "tp")
    query_grad = grads[:PER, :QB].reshape(TOK, 2 * DH)
    by_y = swap(weight_term(target, grads, inputs), "y")
    by_z = call(
        regroup_kernel,
        jax.ShapeDtypeStruct((16, W_ROWS + 4 * SLOT_ROWS, 2 * DH), bf16),
        [by_y],
        name="regroup",
    )
    by_z = swap(by_z, "z")
    keyval_grad, weight_grad = call(
        home_kernel,
        [
            jax.ShapeDtypeStruct((OWN * PIECE, 2 * DH), jnp.float32),
            jax.ShapeDtypeStruct((W_ROWS, 2 * DH), jnp.float32),
        ],
        [slots, by_z, grads],
        name="home",
    )
    return query_grad, keyval_grad.reshape(OWN, PIECE, 2 * DH), weight_grad


def solution(mesh):
    split = Mesh(mesh.devices.reshape(16, 4, TP), ("z", "y", "tp"))
    kv = ("z", "y")
    return jax.shard_map(
        body,
        mesh=split,
        in_specs=(P(kv, "tp"), P(kv, None), P("tp", kv), P(kv, "tp"), P(kv, None), P()),
        out_specs=(P(kv, "tp"), P(kv, "tp", None), P(kv, "tp")),
        check_vma=False,
    )
```

time: 166 us -> 122 us (0.73)
  the two profiles are of different devices: /device:TPU:2 before, /device:TPU:32 now
where the time goes in v2:
time: 122 us; the launch traced here: 121 us
  waiting for transfers between devices  43.3 us (35%)
  starting transfers between devices  27.4 us (22%)
  blocking collectives  24.7 us (20%)
  Pallas kernels  15.7 us (13%)
  local copies, waits for them, and re-layouts  9.13 us (7%)
    all_to_all x3, waiting for transfers between devices, swap(): return lax.all_to_all(array, axis, 0, 0, tiled=True)  43.3 us
    all_to_all x3, starting transfers between devices, swap(): return lax.all_to_all(array, axis, 0, 0, tiled=True)  27.4 us
    all_to_all x2, blocking collectives, swap(): return lax.all_to_all(array, axis, 0, 0, tiled=True)  24.7 us
    pallas_call x5, Pallas kernels, call(): pl.pallas_call(kernel, out_shape=out_shape, in_specs=[VMEM for _ in args]...  12.3 us
    unnamed x13, local copies, waits for them, and re-layouts  6.39 us
    pallas_call x1, Pallas kernels, weight_term(): pl.pallas_call(weight_kernel, grid=(inputs.shape[1] // tile,), in_specs=[...  3.46 us
  transfers between devices with their start and end apart: 3, of which 3 were waited for; matrix products, arithmetic and copies ran while one was open for 3% of the time, Pallas kernels for 0%

profile of v2, /device:TPU:32, one launch (start us, length us, event | category | flops | bytes accessed | tf_op | source)
XLA Modules:
  0.0 121.3 jit_solution(7352747569661976868)
XLA Ops:
  0.6 0.9 copy-done.1
  1.6 0.8 copy-done.4
  2.3 1.5 %offer.1 = (bf16[512,128]{1,0:T(8,128)(2,1)}, f32[8,512]{1,0:T(8,128)S(1)}) custom-call(s32[16,448]{1,0:T(8,128)S(1)} %bitcast.13, bf16[896,128]{1,0:T(8,128)(2,1)S(1)} %copy-done.1), custom_call_target="tpu_custom_call" | custom-call | tf_op jit(solution)/shard_map/offer/pallas_call | solution.py:40
  3.8 18.4 %all-to-all-start = ((bf16[64,8,128]{2,1,0:T(8,128)(2,1)}), bf16[64,8,128]{2,1,0:T(8,128)(2,1)S(1)}, u32[]{:S(2)}, u32[]{:S(2)}) async-start(bf16[64,8,128]{2,1,0:T(8,128)(2,1)} %bitcast.5), calls=%async_computation | async-start | bytes 262144 | tf_op jit(solution)/shard_map/all_to_all | solution.py:226
  22.2 0.8 dynamic-slice
  23.2 0.2 select_reduce_fusion
  23.7 15.2 %all-to-all-done = bf16[64,8,128]{2,1,0:T(8,128)(2,1)S(1)} async-done(((bf16[64,8,128]{2,1,0:T(8,128)(2,1)}), bf16[64,8,128]{2,1,0:T(8,128)(2,1)S(1)}, u32[]{:S(2)}, u32[]{:S(2)}) %all-to-all-start) | async-done | bytes 131104 | tf_op jit(solution)/shard_map/all_to_all | solution.py:226
  38.9 0.9 copy-done.2
  39.9 0.9 copy-done.3
  40.8 0.7 copy-done.5
  41.5 1.2 pick.1
  42.7 4.3 %all-to-all-start.1 = ((bf16[8,320,128]{2,1,0:T(8,128)(2,1)}), bf16[8,320,128]{2,1,0:T(8,128)(2,1)S(1)}, u32[]{:S(2)}, u32[]{:S(2)}) async-start(bf16[8,320,128]{2,1,0:T(8,128)(2,1)} %pick.1), calls=%async_computation.1 | async-start | bytes 1310720 | tf_op jit(solution)/shard_map/all_to_all | solution.py:226
  47.3 0.8 constant_dynamic-slice_fusion
  48.1 10.6 %all-to-all-done.1.in_ref = bf16[8,320,128]{2,1,0:T(8,128)(2,1)S(1)} async-done(((bf16[8,320,128]{2,1,0:T(8,128)(2,1)}), bf16[8,320,128]{2,1,0:T(8,128)(2,1)S(1)}, u32[]{:S(2)}, u32[]{:S(2)}) %all-to-all-start.1) | async-done | bytes 655392 | tf_op jit(solution)/shard_map/all_to_all | solution.py:226
  58.7 8.1 %attention.1 = bf16[8,192,128]{2,1,0:T(8,128)(2,1)S(1)} custom-call(f32[1,512]{1,0:T(1,128)S(1)} %broadcast_in_dim.54.bias_ref, bf16[8,16,128]{2,1,0:T(8,128)(2,1)S(1)} %bitcast.12, bf16[8,320,128]{2,1,0:T(8,128)(2,1)S(1)} %all-to-all-done.1.in_ref), custom_call_target="tpu_custom_call" | custom-call | tf_op jit(solution)/shard_map/attention/pallas_call | solution.py:40
  66.8 11.3 %all_to_all.25.grad_ref.grads_ref = bf16[8,192,128]{2,1,0:T(8,128)(2,1)S(1)} all-to-all(bf16[8,192,128]{2,1,0:T(8,128)(2,1)S(1)} %attention.1), channel_id=1, replica_groups=mesh['z'=16,'y'=4,'tp'=8] {'tp'}, dimensions={0} | all-to-all | bytes 786432 | tf_op jit(solution)/shard_map/all_to_all | solution.py:226
  78.1 2.0 %copy-done = bf16[896,2048]{1,0:T(8,128)(2,1)S(1)} copy-done((bf16[896,2048]{1,0:T(8,128)(2,1)S(1)}, bf16[896,2048]{1,0:T(8,128)(2,1)}, u32[]{:S(2)}) %copy-start) | copy-done | bytes 3670040
  80.1 3.5 %weight.1 = bf16[4,16,40,128]{3,2,1,0:T(8,128)(2,1)S(1)} custom-call(f32[1,512]{1,0:T(1,128)S(1)} %convert_element_type.6.target_ref, bf16[8,192,128]{2,1,0:T(8,128)(2,1)S(1)} %all_to_all.25.grad_ref.grads_ref, bf16[896,2048]{1,0:T(8,128)(2,1)S(1)} %copy-done), custom_call_target="tpu_custom_call" | custom-call | tf_op jit(solution)/shard_map/weight/pallas_call | solution.py:185
  83.6 13.4 %all_to_all.26.in_ref = bf16[4,16,40,128]{3,2,1,0:T(8,128)(2,1)S(1)} all-to-all(bf16[4,16,40,128]{3,2,1,0:T(8,128)(2,1)S(1)} %weight.1), channel_id=1, replica_groups=mesh['z'=16,'y'=4,'tp'=8] {'y'}, dimensions={0} | all-to-all | bytes 1310720 | tf_op jit(solution)/shard_map/all_to_all | solution.py:226
  97.0 0.8 regroup.1
  97.7 4.7 %all-to-all-start.4 = ((bf16[16,64,128]{2,1,0:T(8,128)(2,1)}), bf16[16,64,128]{2,1,0:T(8,128)(2,1)S(1)}, u32[]{:S(2)}, u32[]{:S(2)}) async-start(bf16[16,64,128]{2,1,0:T(8,128)(2,1)} %regroup.1), calls=%async_computation.4 | async-start | bytes 524288 | tf_op jit(solution)/shard_map/all_to_all | solution.py:226
  102.4 0.7 slice.8
  103.2 17.4 %all-to-all-done.4.returned_ref = bf16[16,64,128]{2,1,0:T(8,128)(2,1)S(1)} async-done(((bf16[16,64,128]{2,1,0:T(8,128)(2,1)}), bf16[16,64,128]{2,1,0:T(8,128)(2,1)S(1)}, u32[]{:S(2)}, u32[]{:S(2)}) %all-to-all-start.4) | async-done | bytes 262176 | tf_op jit(solution)/shard_map/all_to_all | solution.py:226
  120.5 0.8 home.1
  (21 shorter events, 0.8 us)
Async XLA Ops:
  0.6 0.9 copy-start.1
  1.6 0.8 copy-start.4
  3.8 35.1 %all-to-all-start = ((bf16[64,8,128]{2,1,0:T(8,128)(2,1)}), bf16[64,8,128]{2,1,0:T(8,128)(2,1)S(1)}, u32[]{:S(2)}, u32[]{:S(2)}) async-start(bf16[64,8,128]{2,1,0:T(8,128)(2,1)} %bitcast.5), calls=%async_computation | async-start | bytes 262144 | tf_op jit(solution)/shard_map/all_to_all | solution.py:226
  38.9 0.9 copy-start.2
  39.9 0.9 copy-start.3
  40.8 0.7 copy-start.5
  42.7 16.0 %all-to-all-start.1 = ((bf16[8,320,128]{2,1,0:T(8,128)(2,1)}), bf16[8,320,128]{2,1,0:T(8,128)(2,1)S(1)}, u32[]{:S(2)}, u32[]{:S(2)}) async-start(bf16[8,320,128]{2,1,0:T(8,128)(2,1)} %pick.1), calls=%async_computation.1 | async-start | bytes 1310720 | tf_op jit(solution)/shard_map/all_to_all | solution.py:226
  78.1 2.0 %copy-start = (bf16[896,2048]{1,0:T(8,128)(2,1)S(1)}, bf16[896,2048]{1,0:T(8,128)(2,1)}, u32[]{:S(2)}) copy-start(bf16[896,2048]{1,0:T(8,128)(2,1)} %in_ref.1) | copy-start | bytes 11010052
  97.7 22.8 %all-to-all-start.4 = ((bf16[16,64,128]{2,1,0:T(8,128)(2,1)}), bf16[16,64,128]{2,1,0:T(8,128)(2,1)S(1)}, u32[]{:S(2)}, u32[]{:S(2)}) async-start(bf16[16,64,128]{2,1,0:T(8,128)(2,1)} %regroup.1), calls=%async_computation.4 | async-start | bytes 524288 | tf_op jit(solution)/shard_map/all_to_all | solution.py:226
